TPU v7x, 512 devices: a whole 4x8x8 slice. The times are simulated.
512 devices in a mesh: sp: 32 (over z, x), tp: 16 (over y, core).
Axes of the slice: x: 4, y: 8, z: 8, core: 2. Of those that a mesh axis runs over, the one named last changes fastest.
Arguments:
- queries: bfloat16 [8192, 2048], P('sp', 'tp'), may hold values from -6 to 6
- key_matrix: bfloat16 [8192, 2048], P('sp', 'tp'), may hold values from -6 to 6
- value_matrix: bfloat16 [8192, 4096], P('sp', 'tp'), may hold values from -6 to 6
- output_gate_preactivation: bfloat16 [8192, 4096], P('sp', 'tp'), may hold values from -6 to 6
- decay_preactivation: bfloat16 [8192, 2048], P('sp', 'tp')
- extra_log_decay: float32 [8192, 16], P('sp', 'tp'), may hold values from -0.7 to 0
- head_norm_gain: bfloat16 [256], replicated, may hold values from 0.099609375 to 1.8984375
- output_projection: bfloat16 [4096, 2048], P(None, 'tp'), may hold values from -0.09375 to 0.09375
- residual: bfloat16 [8192, 2048], P('sp', 'tp'), may hold values from -210 to 210
- feedforward_gain: bfloat16 [2048], replicated, may hold values from 0.099609375 to 1.8984375
- routing: int32 [8192, 4], P('sp'), may hold values from 0 to 127, all different within a row; in each aligned block of 256 rows (0 to 255, 256 to 511, ...) at most 12 rows name the same one
- router_score: float32 [8192, 4], P('sp'), may hold values from 0.05 to 1
- expert_gate_weight: bfloat16 [2048, 131072], P(None, ('sp', 'tp')), may hold values from -0.125 to 0.125
- expert_up_weight: bfloat16 [2048, 131072], P(None, ('sp', 'tp')), may hold values from -0.125 to 0.125
- expert_down_weight: bfloat16 [131072, 2048], P(('sp', 'tp')), may hold values from -0.1875 to 0.1875
- shared_expert_gate: bfloat16 [2048, 512], P(None, 'tp'), may hold values from -0.125 to 0.125
- shared_expert_up: bfloat16 [2048, 512], P(None, 'tp'), may hold values from -0.125 to 0.125
- shared_expert_down: bfloat16 [512, 2048], P(None, 'tp'), may hold values from -0.25 to 0.25
Outputs:
- layer_out: bfloat16 [8192, 2048], P('sp', 'tp')
Inputs may be any that keep to these rules, and one draw needn't show every extreme that they name: `routing`: each row names 4 different experts. In each aligned block of 256 rows, the rows of one index of sp, no expert is named by more than 12 rows, a bound that some expert reaches in some blocks.
All inputs are finite; a program needn't handle non-finite values.
Results may differ from a plain program's by a relative error of at most 0.01.
Values may be sent and summed in bfloat16 or wider, within the bound.
No kernel may reach another device: no remote copies, remote signals or barrier semaphores. Data moves between devices by JAX's collectives and lax.ppermute only.
A program may use at most 64 MiB of HBM per device.

v0:
```python
import jax
import jax.numpy as jnp
from jax import lax
from jax.sharding import Mesh
from jax.sharding import PartitionSpec as P

DK = 128
DV = 256
BLOCK_POSITIONS = 64
FF_PARTS = 4
SP = ("sp_0", "sp_1")
SP_TP = ("sp_0", "sp_1", "tp")
HIGHEST = lax.Precision.HIGHEST
EPSILON = 1e-06
ROUTE_SCALE = 2.5
GATE_TEMPER = 16.0


def nothing_yet(value, identity):
    return jax.tree.map(
        lambda part, zero: jnp.zeros_like(part) + jnp.asarray(zero, part.dtype), value, identity
    )


def prefix_by_axis(value, axes, combine, identity):
    before = start = nothing_yet(value, identity)
    total = value
    for axis in reversed(axes):
        count, position = (lax.axis_size(axis), lax.axis_index(axis))
        pieces = jax.tree.map(
            lambda part, kind: lax.all_gather(part.astype(kind), axis),
            total,
            (jnp.bfloat16, jnp.bfloat16),
        )
        inside, total = (start, start)
        for k in range(count):
            passed = k < position
            total = combine(
                total, jax.tree.map(lambda part, own: part[k].astype(own.dtype), pieces, value)
            )
            inside = jax.tree.map(lambda new, old: jnp.where(passed, new, old), total, inside)
        before = combine(inside, before)
    return before


def laid_out(blocks, dim):
    blocks = jnp.moveaxis(blocks, 0, dim)
    dims = blocks.shape
    return blocks.reshape(*dims[:dim], dims[dim] * dims[dim + 1], *dims[dim + 2 :])


def sent_to_all(value, axis):
    copies = jnp.broadcast_to(value, (lax.axis_size(axis), *value.shape))
    return lax.all_to_all(copies, axis, split_axis=0, concat_axis=0, tiled=True)


def gather_directly(value, axis, dim):
    return laid_out(sent_to_all(value, axis), dim)


def from_partner(value, axis, bit):
    mask = 2**bit
    pairs = [(source, source ^ mask) for source in range(lax.axis_size(axis))]
    return lax.ppermute(value, axis, pairs)


def carry_combine(first_part, second_part):
    return (
        first_part[0] * second_part[0],
        second_part[0][..., None] * first_part[1] + second_part[1],
    )


def attention_heads(queries, key_matrix, value_matrix, decay_preactivation, extra_log_decay):
    tokens = queries.shape[0]
    local_head_count = extra_log_decay.shape[1]
    block_count = tokens // BLOCK_POSITIONS
    query_block = queries.astype(jnp.float32).reshape(
        block_count, BLOCK_POSITIONS, local_head_count, DK
    ) * DK ** (-0.5)
    key_block = key_matrix.astype(jnp.float32).reshape(
        block_count, BLOCK_POSITIONS, local_head_count, DK
    )
    value_block = value_matrix.astype(jnp.float32).reshape(
        block_count, BLOCK_POSITIONS, local_head_count, DV
    )
    log_decay_rows = (
        jax.nn.log_sigmoid(decay_preactivation.astype(jnp.float32)).reshape(
            block_count, BLOCK_POSITIONS, local_head_count, DK
        )
        / GATE_TEMPER
    )
    log_decay_rows = (
        log_decay_rows
        + extra_log_decay.reshape(block_count, BLOCK_POSITIONS, local_head_count)[..., None]
    )
    inside = jnp.cumsum(log_decay_rows, axis=1)
    block_total = inside[:, -1]
    query_decay = query_block * jnp.exp(inside)
    key_decay = key_block * jnp.exp(-inside)
    causal = jnp.tril(jnp.ones((BLOCK_POSITIONS, BLOCK_POSITIONS), dtype=bool))
    scores = jnp.where(
        causal, jnp.einsum("nthd,nshd->nhts", query_decay, key_decay, precision=HIGHEST), 0.0
    )
    within = jnp.einsum("nhts,nshv->nthv", scores, value_block, precision=HIGHEST)
    key_end = key_block * jnp.exp(block_total[:, None] - inside)
    update = jnp.einsum("nshd,nshv->nhdv", key_end, value_block, precision=HIGHEST)
    before = jnp.cumsum(block_total, axis=0) - block_total
    ending = jnp.concatenate([before, (before[-1] + block_total[-1])[None]], axis=0)
    after_block = before + block_total
    earlier_mask = jnp.arange(block_count + 1)[:, None] > jnp.arange(block_count)[None, :]
    span_logs = jnp.where(
        earlier_mask[:, :, None, None], ending[:, None] - after_block[None], -1e30
    )
    states = jnp.einsum("nmhd,mhdv->nhdv", jnp.exp(span_logs), update, precision=HIGHEST)
    passed = jnp.einsum("nthd,nhdv->nthv", query_decay, states[:block_count], precision=HIGHEST)
    query_start = query_block * jnp.exp(inside + before[:, None])
    return (within + passed, query_start, jnp.exp(ending[block_count]), states[block_count])


def body(
    queries,
    key_matrix,
    value_matrix,
    output_gate_preactivation,
    decay_preactivation,
    extra_log_decay,
    head_norm_gain,
    output_projection,
    residual,
    feedforward_gain,
    routing,
    router_score,
    expert_gate_weight,
    expert_up_weight,
    expert_down_weight,
    shared_expert_gate,
    shared_expert_up,
    shared_expert_down,
):
    tokens = queries.shape[0]
    local_head_count = extra_log_decay.shape[1]
    local_part, query_start, dev_decay, dev_update = attention_heads(
        queries, key_matrix, value_matrix, decay_preactivation, extra_log_decay
    )
    _, entering = prefix_by_axis(
        (dev_decay, dev_update),
        SP,
        carry_combine,
        (jnp.ones_like(dev_decay), jnp.zeros_like(dev_update)),
    )
    attention_output = local_part + jnp.einsum(
        "nthd,hdv->nthv", query_start, entering, precision=HIGHEST
    )
    attention_output = attention_output.reshape(tokens, local_head_count, DV)
    inverse_rms = lax.rsqrt(
        jnp.mean(attention_output * attention_output, axis=-1, keepdims=True) + EPSILON
    )
    gate_act = jax.nn.silu(
        output_gate_preactivation.astype(jnp.float32).reshape(tokens, local_head_count, DV)
    )
    head_rows = (
        (attention_output * inverse_rms * head_norm_gain.astype(jnp.float32) * gate_act)
        .reshape(tokens, local_head_count * DV)
        .astype(jnp.bfloat16)
    )
    projected = jnp.dot(
        lax.all_gather(head_rows, "tp", axis=1, tiled=True),
        output_projection,
        preferred_element_type=jnp.float32,
    )
    mid_local = (residual.astype(jnp.float32) + projected).astype(jnp.bfloat16)
    mid_rows = gather_directly(mid_local, "tp", 1).astype(jnp.float32)
    normed = (
        mid_rows
        * lax.rsqrt(jnp.mean(mid_rows * mid_rows, axis=-1, keepdims=True) + EPSILON)
        * feedforward_gain.astype(jnp.float32)
    ).astype(jnp.bfloat16)
    shared_pre = jnp.dot(normed, shared_expert_gate, preferred_element_type=jnp.float32)
    shared_lin = jnp.dot(normed, shared_expert_up, preferred_element_type=jnp.float32)
    shared_hidden = (jax.nn.silu(shared_pre) * shared_lin).astype(jnp.bfloat16)
    senders = lax.axis_size(SP)
    tp_count = lax.axis_size("tp")
    tp_bits = tp_count.bit_length() - 1
    tp_index = lax.axis_index("tp")
    groups = tp_count // FF_PARTS
    group_here = tp_index // FF_PARTS
    part_here = tp_index % FF_PARTS
    model_width = normed.shape[1]
    picks = routing.shape[1]
    expert_total = senders * groups
    rows_most = max(2, 3 * tokens * picks // (2 * expert_total))
    slot_count = senders * rows_most
    flat_expert = routing.reshape(-1)
    one_hot = (flat_expert[:, None] == jnp.arange(expert_total, dtype=jnp.int32)[None, :]).astype(
        jnp.int32
    )
    rank_before = jnp.sum((jnp.cumsum(one_hot, axis=0) - one_hot) * one_hot, axis=1)
    owned = flat_expert % groups == group_here
    slot_index = jnp.where(owned, flat_expert // groups * rows_most + rank_before, slot_count)
    token_index = jnp.arange(flat_expert.shape[0], dtype=jnp.int32) // picks
    part_width = model_width // FF_PARTS
    normed_part = lax.dynamic_slice_in_dim(normed, part_here * part_width, part_width, 1)
    outgoing = (
        jnp.zeros((slot_count, part_width), jnp.bfloat16)
        .at[slot_index]
        .set(normed_part[token_index], mode="drop")
    )
    arrived = lax.all_to_all(
        outgoing.reshape(senders, rows_most, part_width),
        SP,
        split_axis=0,
        concat_axis=0,
        tiled=True,
    )
    for bit in range(2):
        partner_cols = from_partner(arrived, "tp", bit)
        upper = (tp_index >> bit) % 2
        arrived = jnp.where(
            upper == 1,
            jnp.concatenate([partner_cols, arrived], axis=2),
            jnp.concatenate([arrived, partner_cols], axis=2),
        )
    rows_in = arrived.reshape(slot_count, model_width)
    gate_pre = jnp.dot(rows_in, expert_gate_weight, preferred_element_type=jnp.float32)
    up_pre = jnp.dot(rows_in, expert_up_weight, preferred_element_type=jnp.float32)
    routed_hidden = (jax.nn.silu(gate_pre) * up_pre).astype(jnp.bfloat16)
    partial_out = jnp.dot(routed_hidden, expert_down_weight, preferred_element_type=jnp.float32)
    slab_width = model_width // tp_count
    partial_out = partial_out.reshape(slot_count, groups, FF_PARTS, slab_width)
    for bit in (1, 0):
        paired = partial_out.reshape(slot_count, groups, 2, 2**bit, slab_width)
        upper = (tp_index >> bit) % 2
        kept = lax.dynamic_index_in_dim(paired, upper, 2, keepdims=False)
        given = lax.dynamic_index_in_dim(paired, 1 - upper, 2, keepdims=False)
        partial_out = kept + from_partner(given.astype(jnp.bfloat16), "tp", bit).astype(given.dtype)
    expert_out = partial_out.reshape(senders, rows_most, groups, slab_width).astype(jnp.bfloat16)
    shared_out = jnp.dot(
        lax.all_gather(shared_hidden, "tp", axis=1, tiled=True),
        shared_expert_down,
        preferred_element_type=jnp.float32,
    )
    returned = lax.all_to_all(expert_out, SP, split_axis=0, concat_axis=0, tiled=True).reshape(
        slot_count, groups, slab_width
    )
    safe_slot = jnp.minimum(slot_index, slot_count - 1)
    route_weight = ROUTE_SCALE * router_score / jnp.sum(router_score, axis=1, keepdims=True)
    pair_weight = jnp.where(owned, route_weight.reshape(-1), 0.0)
    picked = returned[safe_slot].astype(jnp.float32) * pair_weight[:, None, None]
    routed_part = jnp.sum(picked.reshape(tokens, picks, groups, slab_width), axis=1)
    for bit in range(tp_bits - 1, 1, -1):
        paired = routed_part.reshape(tokens, 2, 2 ** (bit - 2), slab_width)
        upper = (tp_index >> bit) % 2
        kept = lax.dynamic_index_in_dim(paired, upper, 1, keepdims=False)
        given = lax.dynamic_index_in_dim(paired, 1 - upper, 1, keepdims=False)
        routed_part = kept + from_partner(given.astype(jnp.bfloat16), "tp", bit).astype(given.dtype)
    routed = routed_part.reshape(tokens, slab_width)
    return (mid_local.astype(jnp.float32) + routed + shared_out).astype(jnp.bfloat16)


def solution(mesh):
    finer = Mesh(mesh.devices.reshape(8, 4, mesh.shape["tp"]), ("sp_0", "sp_1", "tp"))
    in_specs = (
        P(SP, "tp"),
        P(SP, "tp"),
        P(SP, "tp"),
        P(SP, "tp"),
        P(SP, "tp"),
        P(SP, "tp"),
        P(),
        P(None, "tp"),
        P(SP, "tp"),
        P(),
        P(SP, None),
        P(SP, None),
        P(None, SP_TP),
        P(None, SP_TP),
        P(SP_TP, None),
        P(None, "tp"),
        P(None, "tp"),
        P(None, "tp"),
    )
    out_specs = P(SP, "tp")
    return jax.shard_map(body, mesh=finer, in_specs=in_specs, out_specs=out_specs, check_vma=False)
```

profile of v0, /device:TPU:1, one launch (start us, length us, event | category | flops | bytes accessed | tf_op | source)
XLA Modules:
  0.0 347.6 jit_solution(1330581877182747626)
XLA Ops:
  13.6 8.5 %all_gather.22 = bf16[4,1,128]{2,1,0:T(2,128)(2,1)S(1)} all-gather(bf16[1,1,128]{2,1,0:T(2,128)(2,1)S(1)} %get-tuple-element.7), channel_id=1, replica_groups=mesh['sp_0'=8,'sp_1'=4,'tp'=16] {'sp_1'}, dimensions={0}, use_global_device_ids=true | all-gather | bytes 1280 | tf_op jit(solution)/shard_map/all_gather | solution.py:31
  22.1 18.6 %all_gather.23 = bf16[8,1,128]{2,1,0:T(2,128)(2,1)S(1)} all-gather(bf16[1,1,128]{2,1,0:T(2,128)(2,1)S(1)} %multiply_convert_fusion.1), channel_id=1, replica_groups=mesh['sp_0'=8,'sp_1'=4,'tp'=16] {'sp_0'}, dimensions={0}, use_global_device_ids=true | all-gather | bytes 2304 | tf_op jit(solution)/shard_map/all_gather | solution.py:31
  42.6 9.4 %all_gather.24 = bf16[4,1,128,256]{3,2,1,0:T(8,128)(2,1)S(1)} all-gather(bf16[1,1,128,256]{3,2,1,0:T(8,128)(2,1)S(1)} %copy.45), channel_id=1, replica_groups=mesh['sp_0'=8,'sp_1'=4,'tp'=16] {'sp_1'}, dimensions={0}, use_global_device_ids=true | all-gather | bytes 327680 | tf_op jit(solution)/shard_map/all_gather | solution.py:31
  52.6 21.8 %all_gather.25 = bf16[8,1,128,256]{3,2,1,0:T(8,128)(2,1)} all-gather(bf16[1,1,128,256]{3,2,1,0:T(8,128)(2,1)S(1)} %fusion.46), channel_id=1, replica_groups=mesh['sp_0'=8,'sp_1'=4,'tp'=16] {'sp_0'}, dimensions={0}, use_global_device_ids=true | all-gather | bytes 589824 | tf_op jit(solution)/shard_map/all_gather | solution.py:31
  79.1 53.5 %all-gather.2.cloned.1.call-done = bf16[256,4096]{1,0:T(8,128)(2,1)} async-done(((bf16[256,256]{1,0:T(8,128)(2,1)}), bf16[256,4096]{1,0:T(8,128)(2,1)}) %all-gather.2.cloned.1.call-update) | async-done | bytes 2097168 | tf_op jit(solution)/shard_map/all_gather | solution.py:168
  132.6 2.3 fusion.6
  136.7 5.1 %all-to-all-start = ((bf16[16,256,128]{2,1,0:T(8,128)(2,1)}), bf16[16,256,128]{2,1,0:T(8,128)(2,1)S(1)}, u32[]{:S(2)}, u32[]{:S(2)}) async-start(bf16[16,256,128]{2,1,0:T(8,128)(2,1)} %broadcast_in_dim.52), calls=%async_computation | async-start | bytes 2097152 | tf_op jit(solution)/shard_map/all_to_all | solution.py:54
  143.4 26.5 %all-to-all-done = bf16[16,256,128]{2,1,0:T(8,128)(2,1)S(1)} async-done(((bf16[16,256,128]{2,1,0:T(8,128)(2,1)}), bf16[16,256,128]{2,1,0:T(8,128)(2,1)S(1)}, u32[]{:S(2)}, u32[]{:S(2)}) %all-to-all-start) | async-done | bytes 1048608 | tf_op jit(solution)/shard_map/all_to_all | solution.py:54
  170.5 9.7 %scatter_custom_fusion = bf16[384,512]{1,0:T(8,128)(2,1)S(1)} fusion(s32[1024]{0:T(1024)S(1)} %bitcast.324, bf16[256,512]{1,0:T(8,128)(2,1)S(1)} %constant_dynamic-slice_fusion.2, s32[1024]{0:T(1024)S(1)} %broadcast_clamp_fusion.1, bf16[]{:T(256)} %constant.181.clone.1), kind=kCustom, calls=%fused_computation.26 | custom fusion | bytes 393218 | tf_op jit(solution)/shard_map/scatter | solution.py:207
  180.3 27.1 %all_to_all.15 = bf16[32,12,512]{2,1,0:T(8,128)(2,1)S(1)} all-to-all(bf16[32,12,512]{2,1,0:T(8,128)(2,1)S(1)} %reshape.1386), channel_id=1, replica_groups=mesh['sp_0'=8,'sp_1'=4,'tp'=16] {'sp_0','sp_1'}, dimensions={0} | all-to-all | bytes 786432 | tf_op jit(solution)/shard_map/all_to_all | solution.py:209
  216.3 17.7 %collective-permute-done.1 = bf16[32,12,1024]{2,0,1:T(8,128)(2,1)} collective-permute-done((bf16[32,12,1024]{2,0,1:T(8,128)(2,1)}, bf16[32,12,1024]{2,0,1:T(8,128)(2,1)}, u32[]{:S(2)}, u32[]{:S(2)}) %collective-permute-start.1) | collective-permute-done | bytes 786464 | tf_op jit(solution)/shard_map/ppermute | solution.py:64
  236.7 2.8 fusion.18
  239.5 5.1 %fusion.19 = f32[384,2048]{1,0:T(8,128)} fusion(bf16[256,2048]{1,0:T(8,128)(2,1)S(1)} %copy-done, f32[384,256]{1,0:T(8,128)S(1)} %fusion.18, bf16[2048,256]{1,0:T(8,128)(2,1)} %param.31, bf16[384,1024]{1,0:T(8,128)(2,1)} %maximum_select_fusion.2, bf16[384,1024]{1,0:T(8,128)(2,1)S(1)} %copy-done.3, pred[]{:T(512)S(6)} %eq.66), kind=kOutput, calls=%fused_computation.48 | convolution fusion | flops 812974080 | bytes 7208961 | tf_op jit(solution)/shard_map/dot_general | solution.py:228
  244.7 5.6 %reshape_reshape.3 = f32[384,4,2,2,128]{4,3,2,1,0:T(2,128)} reshape(f32[384,2048]{1,0:T(8,128)} %fusion.19) | data formatting | bytes 6291456 | tf_op jit(solution)/shard_map/reshape;reshape | solution.py:232
  252.4 2.2 collective-permute-start.2
  256.6 15.9 %collective-permute-done.2 = bf16[384,4,2,128]{3,1,0,2:T(4,128)(2,1)} collective-permute-done((bf16[384,4,2,128]{3,1,0,2:T(4,128)(2,1)S(1)}, bf16[384,4,2,128]{3,1,0,2:T(4,128)(2,1)}, u32[]{:S(2)}, u32[]{:S(2)}) %collective-permute-start.2) | collective-permute-done | bytes 786464 | tf_op jit(solution)/shard_map/ppermute | solution.py:64
  275.6 3.8 %collective-permute-start.3 = (bf16[384,4,1,128]{3,1,0,2:T(4,128)(2,1)S(1)}, bf16[384,4,1,128]{3,1,0,2:T(4,128)(2,1)S(1)}, u32[]{:S(2)}, u32[]{:S(2)}) collective-permute-start(bf16[384,4,1,128]{3,1,0,2:T(4,128)(2,1)S(1)} %dynamic-slice_convert_fusion), channel_id=1, source_target_pairs={{0,1},{1,0},{2,3},{3,2},{4,5},{5,4},{6,7},{7,6},{8,9},{9,8},{10,11... | collective-permute-start | bytes 1179656 | tf_op jit(solution)/shard_map/ppermute | solution.py:64
  282.7 4.3 %all-to-all-start.2 = ((bf16[32,12,4,128]{3,2,1,0:T(4,128)(2,1)}), bf16[32,12,4,128]{3,2,1,0:T(4,128)(2,1)S(1)}, u32[]{:S(2)}, u32[]{:S(2)}) async-start(bf16[32,12,4,128]{3,2,1,0:T(4,128)(2,1)} %bitcast.64), calls=%async_computation.2 | async-start | bytes 786432 | tf_op jit(solution)/shard_map/all_to_all | solution.py:243
  289.0 12.0 %all-to-all-done.2 = bf16[32,12,4,128]{3,2,1,0:T(4,128)(2,1)S(1)} async-done(((bf16[32,12,4,128]{3,2,1,0:T(4,128)(2,1)}), bf16[32,12,4,128]{3,2,1,0:T(4,128)(2,1)S(1)}, u32[]{:S(2)}, u32[]{:S(2)}) %all-to-all-start.2) | async-done | bytes 393248 | tf_op jit(solution)/shard_map/all_to_all | solution.py:243
  300.9 3.6 %gather_fusion = bf16[1024,4,128]{2,1,0:T(4,128)(2,1)S(1)} fusion(bf16[384,4,128]{2,1,0:T(4,128)(2,1)S(1)} %bitcast.299, s32[1024]{0:T(1024)S(1)} %broadcast_clamp_fusion), kind=kCustom, calls=%fused_computation.1 | custom fusion | bytes 2101248 | tf_op jit(solution)/shard_map/gather | solution.py:249
  304.5 2.7 fusion.3
  307.4 4.1 %collective-permute-start.4 = (bf16[256,2,128]{2,0,1:T(8,128)(2,1)S(1)}, bf16[256,2,128]{2,0,1:T(8,128)(2,1)S(1)}, u32[]{:S(2)}, u32[]{:S(2)}) collective-permute-start(bf16[256,2,128]{2,0,1:T(8,128)(2,1)S(1)} %fusion.50), channel_id=1, source_target_pairs={{0,8},{1,9},{2,10},{3,11},{4,12},{5,13},{6,14},{7,15},{8,0},{9,1},... | collective-permute-start | bytes 393224 | tf_op jit(solution)/shard_map/ppermute | solution.py:64
  312.0 19.9 %all_gather.27 = bf16[256,512]{0,1:T(8,128)(2,1)S(1)} all-gather(bf16[256,32]{0,1:T(8,128)(2,1)S(1)} %fusion.7), channel_id=1, replica_groups=mesh['sp_0'=8,'sp_1'=4,'tp'=16] {'tp'}, dimensions={1}, use_global_device_ids=true | all-gather | bytes 278528 | tf_op jit(solution)/shard_map/all_gather | solution.py:239
  334.1 6.0 %collective-permute-done.5 = bf16[256,1,128]{2,0,1:T(8,128)(2,1)S(1)} collective-permute-done((bf16[256,1,128]{2,0,1:T(8,128)(2,1)S(1)}, bf16[256,1,128]{2,0,1:T(8,128)(2,1)S(1)}, u32[]{:S(2)}, u32[]{:S(2)}) %collective-permute-start.5) | collective-permute-done | bytes 65568 | tf_op jit(solution)/shard_map/ppermute | solution.py:64
  (129 shorter events, 45.4 us)
Async XLA Ops:
  6.5 233.0 %copy-start = (bf16[256,2048]{1,0:T(8,128)(2,1)S(1)}, bf16[256,2048]{1,0:T(8,128)(2,1)}, u32[]{:S(2)}) copy-start(bf16[256,2048]{1,0:T(8,128)(2,1)} %param.32) | copy-start | bytes 3145732
  6.5 126.1 %all-gather.2.cloned.1.call-start = ((), (), s32[]{:S(2)}) async-start(), calls=%async_computation.3 | async-start | bytes 2228224 | tf_op jit(solution)/shard_map/all_gather | solution.py:168
  9.9 32.0 %copy-start.12 = (bf16[256,128]{1,0:T(8,128)(2,1)S(1)}, bf16[256,128]{1,0:T(8,128)(2,1)}, u32[]{:S(2)}) copy-start(bf16[256,128]{1,0:T(8,128)(2,1)} %param.18) | copy-start | bytes 196612
  10.2 31.7 %copy-start.7 = (bf16[256,128]{1,0:T(8,128)(2,1)S(1)}, bf16[256,128]{1,0:T(8,128)(2,1)}, u32[]{:S(2)}) copy-start(bf16[256,128]{1,0:T(8,128)(2,1)} %param.19) | copy-start | bytes 196612
  11.6 30.7 %copy-start.6 = (bf16[256,256]{1,0:T(8,128)(2,1)S(1)}, bf16[256,256]{1,0:T(8,128)(2,1)}, u32[]{:S(2)}) copy-start(bf16[256,256]{1,0:T(8,128)(2,1)} %param.20) | copy-start | bytes 393220
  13.3 61.0 %copy-start.18 = (bf16[256]{0:T(256)(128)(2,1)S(1)}, bf16[256]{0:T(256)(128)(2,1)}, u32[]{:S(2)}) copy-start(bf16[256]{0:T(256)(128)(2,1)} %param.24) | copy-start | bytes 1540
  74.9 57.7 %copy-start.2 = (bf16[4096,128]{1,0:T(8,128)(2,1)S(1)}, bf16[4096,128]{1,0:T(8,128)(2,1)}, u32[]{:S(2)}) copy-start(bf16[4096,128]{1,0:T(8,128)(2,1)} %param.25) | copy-start | bytes 3145732
  75.4 57.2 %copy-start.13 = (bf16[256,128]{1,0:T(8,128)(2,1)S(1)}, bf16[256,128]{1,0:T(8,128)(2,1)}, u32[]{:S(2)}) copy-start(bf16[256,128]{1,0:T(8,128)(2,1)} %param.26) | copy-start | bytes 196612
  135.5 6.3 %copy-start.14 = (s32[256,4]{0,1:T(4,128)S(1)}, s32[256,4]{0,1:T(4,128)}, u32[]{:S(2)}) copy-start(s32[256,4]{0,1:T(4,128)} %param.28) | copy-start | bytes 12292
  135.5 6.8 %copy-start.16 = (bf16[2048]{0:T(1024)(128)(2,1)S(1)}, bf16[2048]{0:T(1024)(128)(2,1)}, u32[]{:S(2)}) copy-start(bf16[2048]{0:T(1024)(128)(2,1)} %param.27) | copy-start | bytes 12292
  136.7 33.1 %all-to-all-start = ((bf16[16,256,128]{2,1,0:T(8,128)(2,1)}), bf16[16,256,128]{2,1,0:T(8,128)(2,1)S(1)}, u32[]{:S(2)}, u32[]{:S(2)}) async-start(bf16[16,256,128]{2,1,0:T(8,128)(2,1)} %broadcast_in_dim.52), calls=%async_computation | async-start | bytes 2097152 | tf_op jit(solution)/shard_map/all_to_all | solution.py:54
  207.4 3.8 %collective-permute-start = (bf16[32,12,512]{2,1,0:T(8,128)(2,1)S(1)}, bf16[32,12,512]{2,1,0:T(8,128)(2,1)S(1)}, u32[]{:S(2)}, u32[]{:S(2)}) collective-permute-start(bf16[32,12,512]{2,1,0:T(8,128)(2,1)S(1)} %all_to_all.15), channel_id=1, source_target_pairs={{0,1},{1,0},{2,3},{3,2},{4,5},{5,4},{6,7},{7,6},{8,9},{9,8},{10,11... | collective-permute-start | bytes 1179656 | tf_op jit(solution)/shard_map/ppermute | solution.py:64
  212.9 21.2 %collective-permute-start.1 = (bf16[32,12,1024]{2,0,1:T(8,128)(2,1)}, bf16[32,12,1024]{2,0,1:T(8,128)(2,1)}, u32[]{:S(2)}, u32[]{:S(2)}) collective-permute-start(bf16[32,12,1024]{2,0,1:T(8,128)(2,1)} %copy.52), channel_id=1, source_target_pairs={{0,2},{1,3},{2,0},{3,1},{4,6},{5,7},{6,4},{7,5},{8,10},{9,11},{10,... | collective-permute-start | bytes 2359304 | tf_op jit(solution)/shard_map/ppermute | solution.py:64
  252.4 20.1 %collective-permute-start.2 = (bf16[384,4,2,128]{3,1,0,2:T(4,128)(2,1)S(1)}, bf16[384,4,2,128]{3,1,0,2:T(4,128)(2,1)}, u32[]{:S(2)}, u32[]{:S(2)}) collective-permute-start(bf16[384,4,2,128]{3,1,0,2:T(4,128)(2,1)S(1)} %bitcast.308), channel_id=1, source_target_pairs={{0,2},{1,3},{2,0},{3,1},{4,6},{5,7},{6,4},{7,5},{8,10},{9,11},{10,... | collective-permute-start | bytes 2359304 | tf_op jit(solution)/shard_map/ppermute | solution.py:64
  275.4 11.7 %copy-start.15 = (f32[256,4]{0,1:T(4,128)S(1)}, f32[256,4]{0,1:T(4,128)}, u32[]{:S(2)}) copy-start(f32[256,4]{0,1:T(4,128)} %param.29) | copy-start | bytes 12292
  275.4 12.5 %copy-start.8 = (bf16[2048,32]{0,1:T(8,128)(2,1)S(1)}, bf16[2048,32]{0,1:T(8,128)(2,1)}, u32[]{:S(2)}) copy-start(bf16[2048,32]{0,1:T(8,128)(2,1)} %param.33) | copy-start | bytes 393220
  275.6 5.1 %collective-permute-start.3 = (bf16[384,4,1,128]{3,1,0,2:T(4,128)(2,1)S(1)}, bf16[384,4,1,128]{3,1,0,2:T(4,128)(2,1)S(1)}, u32[]{:S(2)}, u32[]{:S(2)}) collective-permute-start(bf16[384,4,1,128]{3,1,0,2:T(4,128)(2,1)S(1)} %dynamic-slice_convert_fusion), channel_id=1, source_target_pairs={{0,1},{1,0},{2,3},{3,2},{4,5},{5,4},{6,7},{7,6},{8,9},{9,8},{10,11... | collective-permute-start | bytes 1179656 | tf_op jit(solution)/shard_map/ppermute | solution.py:64
  282.7 18.2 %all-to-all-start.2 = ((bf16[32,12,4,128]{3,2,1,0:T(4,128)(2,1)}), bf16[32,12,4,128]{3,2,1,0:T(4,128)(2,1)S(1)}, u32[]{:S(2)}, u32[]{:S(2)}) async-start(bf16[32,12,4,128]{3,2,1,0:T(4,128)(2,1)} %bitcast.64), calls=%async_computation.2 | async-start | bytes 786432 | tf_op jit(solution)/shard_map/all_to_all | solution.py:243
  304.5 7.0 %copy-start.9 = (bf16[2048,32]{0,1:T(8,128)(2,1)S(1)}, bf16[2048,32]{0,1:T(8,128)(2,1)}, u32[]{:S(2)}) copy-start(bf16[2048,32]{0,1:T(8,128)(2,1)} %param.34) | copy-start | bytes 393220
  304.5 7.0 %copy-start.10 = (f32[256,32]{0,1:T(8,128)S(1)}, f32[256,32]{0,1:T(8,128)}, u32[]{:S(2)}) copy-start(f32[256,32]{0,1:T(8,128)} %fusion.143) | copy-start | bytes 98308
  307.3 26.6 %copy-start.11 = (bf16[512,128]{1,0:T(8,128)(2,1)S(1)}, bf16[512,128]{1,0:T(8,128)(2,1)}, u32[]{:S(2)}) copy-start(bf16[512,128]{1,0:T(8,128)(2,1)} %param.35) | copy-start | bytes 393220
  307.3 32.8 %copy-start.5 = (bf16[256,128]{1,0:T(8,128)(2,1)S(1)}, bf16[256,128]{1,0:T(8,128)(2,1)}, u32[]{:S(2)}) copy-start(bf16[256,128]{1,0:T(8,128)(2,1)} %copy-done.4) | copy-start | bytes 196612
  307.4 24.5 %collective-permute-start.4 = (bf16[256,2,128]{2,0,1:T(8,128)(2,1)S(1)}, bf16[256,2,128]{2,0,1:T(8,128)(2,1)S(1)}, u32[]{:S(2)}, u32[]{:S(2)}) collective-permute-start(bf16[256,2,128]{2,0,1:T(8,128)(2,1)S(1)} %fusion.50), channel_id=1, source_target_pairs={{0,8},{1,9},{2,10},{3,11},{4,12},{5,13},{6,14},{7,15},{8,0},{9,1},... | collective-permute-start | bytes 393224 | tf_op jit(solution)/shard_map/ppermute | solution.py:64
  331.9 8.2 %collective-permute-start.5 = (bf16[256,1,128]{2,0,1:T(8,128)(2,1)S(1)}, bf16[256,1,128]{2,0,1:T(8,128)(2,1)S(1)}, u32[]{:S(2)}, u32[]{:S(2)}) collective-permute-start(bf16[256,1,128]{2,0,1:T(8,128)(2,1)S(1)} %dynamic-slice_convert_fusion.2), channel_id=1, source_target_pairs={{0,4},{1,5},{2,6},{3,7},{4,0},{5,1},{6,2},{7,3},{8,12},{9,13},{10,... | collective-permute-start | bytes 196616 | tf_op jit(solution)/shard_map/ppermute | solution.py:64
  (4 other events, 6.6 us)
Sparse Core Ops, SparseCore 0:
  79.2 53.3 all-gather.1
where the time goes:
time: 349 us; the launch traced here: 348 us
  waiting for transfers between devices  135 us (39%)
  blocking collectives  105 us (30%)
  local copies, waits for them, and re-layouts  33.1 us (9%)
  starting transfers between devices  25.5 us (7%)
  matrix products  18 us (5%)
  other arithmetic  16.9 us (5%)
  between operations  14.1 us (4%)
    all_gather x4, blocking collectives, prefix_by_axis(): lax.all_gather(part.astype(kind), axis)  58.2 us
    all_gather x1, waiting for transfers between devices, body(): lax.all_gather(head_rows, 'tp', axis=1, tiled=True)  53.5 us
    ppermute x6, waiting for transfers between devices, from_partner(): return lax.ppermute(value, axis, pairs)  42.8 us
    all_to_all x1, blocking collectives, body(): lax.all_to_all(outgoing.reshape(senders, rows_most, part_width), SP, spli...  27.1 us
    all_to_all x1, waiting for transfers between devices, sent_to_all(): return lax.all_to_all(copies, axis, split_axis=0, concat_axis=0, tiled=True)  26.5 us
    all_gather x1, blocking collectives, body(): lax.all_gather(shared_hidden, 'tp', axis=1, tiled=True)  19.9 us
    ppermute x6, starting transfers between devices, from_partner(): return lax.ppermute(value, axis, pairs)  16.1 us
    all_to_all x1, waiting for transfers between devices, body(): lax.all_to_all(expert_out, SP, split_axis=0, concat_axis=0, tiled=True)  12 us
  transfers between devices with their start and end apart: 9, of which 8 were waited for; matrix products, arithmetic and copies ran while one was open for 2% of the time, Pallas kernels for 0%

commit v1 on v0

--- a/solution.py
+++ b/solution.py
@@ -14,6 +14,11 @@
 EPSILON = 1e-06
 ROUTE_SCALE = 2.5
 GATE_TEMPER = 16.0
+
+
+def gather_by_exchange(value, axis, dim):
+    copies = jnp.concatenate([value] * lax.axis_size(axis), axis=dim)
+    return lax.all_to_all(copies, axis, dim, dim, tiled=True)
 
 
 def nothing_yet(value, identity):
@@ -165,7 +170,7 @@
         .astype(jnp.bfloat16)
     )
     projected = jnp.dot(
-        lax.all_gather(head_rows, "tp", axis=1, tiled=True),
+        gather_by_exchange(head_rows, "tp", 1),
         output_projection,
         preferred_element_type=jnp.float32,
     )

time: 349 us -> 342 us (0.980)
  blocking collectives: 105 us -> 170 us
  waiting for transfers between devices: 135 us -> 80.4 us
  between operations: 14.1 us -> 0.79 us
  other arithmetic: 16.9 us -> 13.1 us
    all_to_all x0 -> x1, blocking collectives: none -> 73.4 us  [gather_by_exchange(): return lax.all_to_all(copies, axis, dim, dim, tiled=True)]
    all_gather x1 -> x0, waiting for transfers between devices: 53.5 us -> none  [body(): lax.all_gather(head_rows, 'tp', axis=1, tiled=True)]
    all_to_all x1, blocking collectives: 27.1 us -> 20.9 us  [body(): lax.all_to_all(outgoing.reshape(senders, rows_most, part_width), SP, spli...]
  transfers between devices with their start and end apart: 9 -> 8, of which waited for: 8 -> 7; matrix products, arithmetic and copies ran while one was open for 2% -> 2% of each run, Pallas kernels for 0% -> 0%
where the time goes in v1:
time: 342 us; the launch traced here: 341 us
  blocking collectives  170 us (50%)
  waiting for transfers between devices  80.4 us (24%)
  local copies, waits for them, and re-layouts  35.7 us (10%)
  starting transfers between devices  24.2 us (7%)
  matrix products  17.2 us (5%)
  other arithmetic  13.1 us (4%)
    all_to_all x1, blocking collectives, gather_by_exchange(): return lax.all_to_all(copies, axis, dim, dim, tiled=True)  73.4 us
    all_gather x4, blocking collectives, prefix_by_axis(): lax.all_gather(part.astype(kind), axis)  55.8 us
    ppermute x6, waiting for transfers between devices, from_partner(): return lax.ppermute(value, axis, pairs)  42.8 us
    all_to_all x1, waiting for transfers between devices, sent_to_all(): return lax.all_to_all(copies, axis, split_axis=0, concat_axis=0, tiled=True)  25.6 us
    all_to_all x1, blocking collectives, body(): lax.all_to_all(outgoing.reshape(senders, rows_most, part_width), SP, spli...  20.9 us
    all_gather x1, blocking collectives, body(): lax.all_gather(shared_hidden, 'tp', axis=1, tiled=True)  19.9 us
    ppermute x6, starting transfers between devices, from_partner(): return lax.ppermute(value, axis, pairs)  16.1 us
    all_to_all x1, waiting for transfers between devices, body(): lax.all_to_all(expert_out, SP, split_axis=0, concat_axis=0, tiled=True)  12 us
  transfers between devices with their start and end apart: 8, of which 7 were waited for; matrix products, arithmetic and copies ran while one was open for 2% of the time, Pallas kernels for 0%

profile of v1, /device:TPU:1, one launch (start us, length us, event | category | flops | bytes accessed | tf_op | source)
XLA Modules:
  0.0 341.5 jit_solution(18419981343144636836)
XLA Ops:
  7.0 8.5 %all_gather.19 = bf16[4,1,128]{2,1,0:T(2,128)(2,1)S(1)} all-gather(bf16[1,1,128]{2,1,0:T(2,128)(2,1)S(1)} %get-tuple-element.7), channel_id=1, replica_groups=mesh['sp_0'=8,'sp_1'=4,'tp'=16] {'sp_1'}, dimensions={0}, use_global_device_ids=true | all-gather | bytes 1280 | tf_op jit(solution)/shard_map/all_gather | solution.py:36
  15.6 18.6 %all_gather.20 = bf16[8,1,128]{2,1,0:T(2,128)(2,1)S(1)} all-gather(bf16[1,1,128]{2,1,0:T(2,128)(2,1)S(1)} %multiply_convert_fusion.1), channel_id=1, replica_groups=mesh['sp_0'=8,'sp_1'=4,'tp'=16] {'sp_0'}, dimensions={0}, use_global_device_ids=true | all-gather | bytes 2304 | tf_op jit(solution)/shard_map/all_gather | solution.py:36
  34.9 9.4 %all_gather.21 = bf16[4,1,128,256]{3,2,1,0:T(8,128)(2,1)S(1)} all-gather(bf16[1,1,128,256]{3,2,1,0:T(8,128)(2,1)S(1)} %copy.65), channel_id=1, replica_groups=mesh['sp_0'=8,'sp_1'=4,'tp'=16] {'sp_1'}, dimensions={0}, use_global_device_ids=true | all-gather | bytes 327680 | tf_op jit(solution)/shard_map/all_gather | solution.py:36
  44.4 19.4 %all_gather.22 = bf16[8,1,128,256]{3,2,1,0:T(8,128)(2,1)S(1)} all-gather(bf16[1,1,128,256]{3,2,1,0:T(8,128)(2,1)S(1)} %fusion.46), channel_id=1, replica_groups=mesh['sp_0'=8,'sp_1'=4,'tp'=16] {'sp_0'}, dimensions={0}, use_global_device_ids=true | all-gather | bytes 589824 | tf_op jit(solution)/shard_map/all_gather | solution.py:36
  65.5 73.4 %all_to_all.24 = bf16[256,16,256]{2,0,1:T(8,128)(2,1)S(1)} all-to-all(bf16[256,16,256]{2,0,1:T(8,128)(2,1)S(1)} %concatenate.34), channel_id=1, replica_groups=mesh['sp_0'=8,'sp_1'=4,'tp'=16] {'tp'}, dimensions={1} | all-to-all | bytes 4194304 | tf_op jit(solution)/shard_map/all_to_all | solution.py:21
  138.9 2.4 copy.66
  141.3 2.6 fusion.6
  145.7 3.7 %all-to-all-start.1 = ((bf16[16,256,128]{2,1,0:T(8,128)(2,1)}), bf16[16,256,128]{2,1,0:T(8,128)(2,1)S(1)}, u32[]{:S(2)}, u32[]{:S(2)}) async-start(bf16[16,256,128]{2,1,0:T(8,128)(2,1)} %broadcast_in_dim.52), calls=%async_computation.1 | async-start | bytes 2097152 | tf_op jit(solution)/shard_map/all_to_all | solution.py:59
  151.0 25.6 %all-to-all-done.1 = bf16[16,256,128]{2,1,0:T(8,128)(2,1)S(1)} async-done(((bf16[16,256,128]{2,1,0:T(8,128)(2,1)}), bf16[16,256,128]{2,1,0:T(8,128)(2,1)S(1)}, u32[]{:S(2)}, u32[]{:S(2)}) %all-to-all-start.1) | async-done | bytes 1048608 | tf_op jit(solution)/shard_map/all_to_all | solution.py:59
  177.2 9.7 %scatter_custom_fusion = bf16[384,512]{1,0:T(8,128)(2,1)S(1)} fusion(s32[1024]{0:T(1024)S(1)} %bitcast.326, bf16[256,512]{1,0:T(8,128)(2,1)S(1)} %constant_dynamic-slice_fusion.2, s32[1024]{0:T(1024)S(1)} %broadcast_clamp_fusion.1, bf16[]{:T(256)} %constant.181.clone.1), kind=kCustom, calls=%fused_computation.26 | custom fusion | bytes 393218 | tf_op jit(solution)/shard_map/scatter | solution.py:212
  187.0 20.9 %all_to_all.25 = bf16[32,12,512]{2,1,0:T(8,128)(2,1)S(1)} all-to-all(bf16[32,12,512]{2,1,0:T(8,128)(2,1)S(1)} %reshape.1406), channel_id=1, replica_groups=mesh['sp_0'=8,'sp_1'=4,'tp'=16] {'sp_0','sp_1'}, dimensions={0} | all-to-all | bytes 786432 | tf_op jit(solution)/shard_map/all_to_all | solution.py:214
  216.9 17.7 %collective-permute-done.1 = bf16[32,12,1024]{2,0,1:T(8,128)(2,1)} collective-permute-done((bf16[32,12,1024]{2,0,1:T(8,128)(2,1)}, bf16[32,12,1024]{2,0,1:T(8,128)(2,1)}, u32[]{:S(2)}, u32[]{:S(2)}) %collective-permute-start.1) | collective-permute-done | bytes 786464 | tf_op jit(solution)/shard_map/ppermute | solution.py:69
  237.3 2.8 fusion.18
  240.1 5.1 %fusion.19 = f32[384,2048]{1,0:T(8,128)} fusion(bf16[256,2048]{1,0:T(8,128)(2,1)S(1)} %copy-done, f32[384,256]{1,0:T(8,128)S(1)} %fusion.18, bf16[2048,256]{1,0:T(8,128)(2,1)} %param.31, bf16[384,1024]{1,0:T(8,128)(2,1)} %maximum_select_fusion.2, bf16[384,1024]{1,0:T(8,128)(2,1)S(1)} %copy-done.2, pred[]{:T(512)S(6)} %eq.66), kind=kOutput, calls=%fused_computation.48 | convolution fusion | flops 812974080 | bytes 7208961 | tf_op jit(solution)/shard_map/dot_general | solution.py:233
  245.3 5.6 %reshape_reshape.3 = f32[384,4,2,2,128]{4,3,2,1,0:T(2,128)} reshape(f32[384,2048]{1,0:T(8,128)} %fusion.19) | data formatting | bytes 6291456 | tf_op jit(solution)/shard_map/reshape;reshape | solution.py:237
  257.2 15.9 %collective-permute-done.2 = bf16[384,4,2,128]{3,1,0,2:T(4,128)(2,1)} collective-permute-done((bf16[384,4,2,128]{3,1,0,2:T(4,128)(2,1)S(1)}, bf16[384,4,2,128]{3,1,0,2:T(4,128)(2,1)}, u32[]{:S(2)}, u32[]{:S(2)}) %collective-permute-start.2) | collective-permute-done | bytes 786464 | tf_op jit(solution)/shard_map/ppermute | solution.py:69
  276.2 3.8 %collective-permute-start.3 = (bf16[384,4,1,128]{3,1,0,2:T(4,128)(2,1)S(1)}, bf16[384,4,1,128]{3,1,0,2:T(4,128)(2,1)S(1)}, u32[]{:S(2)}, u32[]{:S(2)}) collective-permute-start(bf16[384,4,1,128]{3,1,0,2:T(4,128)(2,1)S(1)} %dynamic-slice_convert_fusion), channel_id=1, source_target_pairs={{0,1},{1,0},{2,3},{3,2},{4,5},{5,4},{6,7},{7,6},{8,9},{9,8},{10,11... | collective-permute-start | bytes 1179656 | tf_op jit(solution)/shard_map/ppermute | solution.py:69
  283.4 4.4 %all-to-all-start.3 = ((bf16[32,12,4,128]{3,2,1,0:T(4,128)(2,1)}), bf16[32,12,4,128]{3,2,1,0:T(4,128)(2,1)S(1)}, u32[]{:S(2)}, u32[]{:S(2)}) async-start(bf16[32,12,4,128]{3,2,1,0:T(4,128)(2,1)} %bitcast.65), calls=%async_computation.3 | async-start | bytes 786432 | tf_op jit(solution)/shard_map/all_to_all | solution.py:248
  289.7 12.0 %all-to-all-done.3 = bf16[32,12,4,128]{3,2,1,0:T(4,128)(2,1)S(1)} async-done(((bf16[32,12,4,128]{3,2,1,0:T(4,128)(2,1)}), bf16[32,12,4,128]{3,2,1,0:T(4,128)(2,1)S(1)}, u32[]{:S(2)}, u32[]{:S(2)}) %all-to-all-start.3) | async-done | bytes 393248 | tf_op jit(solution)/shard_map/all_to_all | solution.py:248
  301.7 3.6 %gather_fusion = bf16[1024,4,128]{2,1,0:T(4,128)(2,1)S(1)} fusion(bf16[384,4,128]{2,1,0:T(4,128)(2,1)S(1)} %bitcast.301, s32[1024]{0:T(1024)S(1)} %broadcast_clamp_fusion), kind=kCustom, calls=%fused_computation.1 | custom fusion | bytes 2101248 | tf_op jit(solution)/shard_map/gather | solution.py:254
  305.3 2.7 fusion.3
  308.1 4.2 %collective-permute-start.4 = (bf16[256,2,128]{2,0,1:T(8,128)(2,1)S(1)}, bf16[256,2,128]{2,0,1:T(8,128)(2,1)S(1)}, u32[]{:S(2)}, u32[]{:S(2)}) collective-permute-start(bf16[256,2,128]{2,0,1:T(8,128)(2,1)S(1)} %fusion.50), channel_id=1, source_target_pairs={{0,8},{1,9},{2,10},{3,11},{4,12},{5,13},{6,14},{7,15},{8,0},{9,1},... | collective-permute-start | bytes 393224 | tf_op jit(solution)/shard_map/ppermute | solution.py:69
  312.7 19.9 %all_gather.23 = bf16[256,512]{0,1:T(8,128)(2,1)S(1)} all-gather(bf16[256,32]{0,1:T(8,128)(2,1)S(1)} %fusion.7), channel_id=1, replica_groups=mesh['sp_0'=8,'sp_1'=4,'tp'=16] {'tp'}, dimensions={1}, use_global_device_ids=true | all-gather | bytes 278528 | tf_op jit(solution)/shard_map/all_gather | solution.py:244
  334.9 5.9 %collective-permute-done.5 = bf16[256,1,128]{2,0,1:T(8,128)(2,1)S(1)} collective-permute-done((bf16[256,1,128]{2,0,1:T(8,128)(2,1)S(1)}, bf16[256,1,128]{2,0,1:T(8,128)(2,1)S(1)}, u32[]{:S(2)}, u32[]{:S(2)}) %collective-permute-start.5) | collective-permute-done | bytes 65568 | tf_op jit(solution)/shard_map/ppermute | solution.py:69
  (127 shorter events, 42.9 us)
Async XLA Ops:
  0.0 240.1 %copy-start = (bf16[256,2048]{1,0:T(8,128)(2,1)S(1)}, bf16[256,2048]{1,0:T(8,128)(2,1)}, u32[]{:S(2)}) copy-start(bf16[256,2048]{1,0:T(8,128)(2,1)} %param.32) | copy-start | bytes 3145732
  3.3 30.9 %copy-start.12 = (bf16[256,128]{1,0:T(8,128)(2,1)S(1)}, bf16[256,128]{1,0:T(8,128)(2,1)}, u32[]{:S(2)}) copy-start(bf16[256,128]{1,0:T(8,128)(2,1)} %param.18) | copy-start | bytes 196612
  3.7 30.6 %copy-start.6 = (bf16[256,128]{1,0:T(8,128)(2,1)S(1)}, bf16[256,128]{1,0:T(8,128)(2,1)}, u32[]{:S(2)}) copy-start(bf16[256,128]{1,0:T(8,128)(2,1)} %param.19) | copy-start | bytes 196612
  5.1 29.5 %copy-start.5 = (bf16[256,256]{1,0:T(8,128)(2,1)S(1)}, bf16[256,256]{1,0:T(8,128)(2,1)}, u32[]{:S(2)}) copy-start(bf16[256,256]{1,0:T(8,128)(2,1)} %param.20) | copy-start | bytes 393220
  6.8 57.0 %copy-start.17 = (bf16[256]{0:T(256)(128)(2,1)S(1)}, bf16[256]{0:T(256)(128)(2,1)}, u32[]{:S(2)}) copy-start(bf16[256]{0:T(256)(128)(2,1)} %param.24) | copy-start | bytes 1540
  44.4 20.8 %copy-start.10 = (bf16[256,256]{1,0:T(8,128)(2,1)S(1)}, bf16[256,256]{1,0:T(8,128)(2,1)}, u32[]{:S(2)}) copy-start(bf16[256,256]{1,0:T(8,128)(2,1)} %param.21) | copy-start | bytes 393220
  138.9 2.4 copy-start.13
  144.5 4.9 %copy-start.14 = (s32[256,4]{0,1:T(4,128)S(1)}, s32[256,4]{0,1:T(4,128)}, u32[]{:S(2)}) copy-start(s32[256,4]{0,1:T(4,128)} %param.28) | copy-start | bytes 12292
  144.5 5.4 %copy-start.16 = (bf16[2048]{0:T(1024)(128)(2,1)S(1)}, bf16[2048]{0:T(1024)(128)(2,1)}, u32[]{:S(2)}) copy-start(bf16[2048]{0:T(1024)(128)(2,1)} %param.27) | copy-start | bytes 12292
  145.7 30.9 %all-to-all-start.1 = ((bf16[16,256,128]{2,1,0:T(8,128)(2,1)}), bf16[16,256,128]{2,1,0:T(8,128)(2,1)S(1)}, u32[]{:S(2)}, u32[]{:S(2)}) async-start(bf16[16,256,128]{2,1,0:T(8,128)(2,1)} %broadcast_in_dim.52), calls=%async_computation.1 | async-start | bytes 2097152 | tf_op jit(solution)/shard_map/all_to_all | solution.py:59
  208.0 3.8 %collective-permute-start = (bf16[32,12,512]{2,1,0:T(8,128)(2,1)S(1)}, bf16[32,12,512]{2,1,0:T(8,128)(2,1)S(1)}, u32[]{:S(2)}, u32[]{:S(2)}) collective-permute-start(bf16[32,12,512]{2,1,0:T(8,128)(2,1)S(1)} %all_to_all.25), channel_id=1, source_target_pairs={{0,1},{1,0},{2,3},{3,2},{4,5},{5,4},{6,7},{7,6},{8,9},{9,8},{10,11... | collective-permute-start | bytes 1179656 | tf_op jit(solution)/shard_map/ppermute | solution.py:69
  213.5 21.2 %collective-permute-start.1 = (bf16[32,12,1024]{2,0,1:T(8,128)(2,1)}, bf16[32,12,1024]{2,0,1:T(8,128)(2,1)}, u32[]{:S(2)}, u32[]{:S(2)}) collective-permute-start(bf16[32,12,1024]{2,0,1:T(8,128)(2,1)} %copy.73), channel_id=1, source_target_pairs={{0,2},{1,3},{2,0},{3,1},{4,6},{5,7},{6,4},{7,5},{8,10},{9,11},{10,... | collective-permute-start | bytes 2359304 | tf_op jit(solution)/shard_map/ppermute | solution.py:69
  237.3 2.8 copy-start.2
  253.1 20.1 %collective-permute-start.2 = (bf16[384,4,2,128]{3,1,0,2:T(4,128)(2,1)S(1)}, bf16[384,4,2,128]{3,1,0,2:T(4,128)(2,1)}, u32[]{:S(2)}, u32[]{:S(2)}) collective-permute-start(bf16[384,4,2,128]{3,1,0,2:T(4,128)(2,1)S(1)} %bitcast.310), channel_id=1, source_target_pairs={{0,2},{1,3},{2,0},{3,1},{4,6},{5,7},{6,4},{7,5},{8,10},{9,11},{10,... | collective-permute-start | bytes 2359304 | tf_op jit(solution)/shard_map/ppermute | solution.py:69
  276.1 11.8 %copy-start.15 = (f32[256,4]{0,1:T(4,128)S(1)}, f32[256,4]{0,1:T(4,128)}, u32[]{:S(2)}) copy-start(f32[256,4]{0,1:T(4,128)} %param.29) | copy-start | bytes 12292
  276.1 12.6 %copy-start.7 = (bf16[2048,32]{0,1:T(8,128)(2,1)S(1)}, bf16[2048,32]{0,1:T(8,128)(2,1)}, u32[]{:S(2)}) copy-start(bf16[2048,32]{0,1:T(8,128)(2,1)} %param.33) | copy-start | bytes 393220
  276.2 5.1 %collective-permute-start.3 = (bf16[384,4,1,128]{3,1,0,2:T(4,128)(2,1)S(1)}, bf16[384,4,1,128]{3,1,0,2:T(4,128)(2,1)S(1)}, u32[]{:S(2)}, u32[]{:S(2)}) collective-permute-start(bf16[384,4,1,128]{3,1,0,2:T(4,128)(2,1)S(1)} %dynamic-slice_convert_fusion), channel_id=1, source_target_pairs={{0,1},{1,0},{2,3},{3,2},{4,5},{5,4},{6,7},{7,6},{8,9},{9,8},{10,11... | collective-permute-start | bytes 1179656 | tf_op jit(solution)/shard_map/ppermute | solution.py:69
  283.4 18.3 %all-to-all-start.3 = ((bf16[32,12,4,128]{3,2,1,0:T(4,128)(2,1)}), bf16[32,12,4,128]{3,2,1,0:T(4,128)(2,1)S(1)}, u32[]{:S(2)}, u32[]{:S(2)}) async-start(bf16[32,12,4,128]{3,2,1,0:T(4,128)(2,1)} %bitcast.65), calls=%async_computation.3 | async-start | bytes 786432 | tf_op jit(solution)/shard_map/all_to_all | solution.py:248
  305.2 7.1 %copy-start.8 = (bf16[2048,32]{0,1:T(8,128)(2,1)S(1)}, bf16[2048,32]{0,1:T(8,128)(2,1)}, u32[]{:S(2)}) copy-start(bf16[2048,32]{0,1:T(8,128)(2,1)} %param.34) | copy-start | bytes 393220
  305.2 7.1 %copy-start.9 = (f32[256,32]{0,1:T(8,128)S(1)}, f32[256,32]{0,1:T(8,128)}, u32[]{:S(2)}) copy-start(f32[256,32]{0,1:T(8,128)} %fusion.143) | copy-start | bytes 98308
  308.0 26.6 %copy-start.11 = (bf16[512,128]{1,0:T(8,128)(2,1)S(1)}, bf16[512,128]{1,0:T(8,128)(2,1)}, u32[]{:S(2)}) copy-start(bf16[512,128]{1,0:T(8,128)(2,1)} %param.35) | copy-start | bytes 393220
  308.0 32.8 %copy-start.4 = (bf16[256,128]{1,0:T(8,128)(2,1)S(1)}, bf16[256,128]{1,0:T(8,128)(2,1)}, u32[]{:S(2)}) copy-start(bf16[256,128]{1,0:T(8,128)(2,1)} %copy-done.3) | copy-start | bytes 196612
  308.1 24.5 %collective-permute-start.4 = (bf16[256,2,128]{2,0,1:T(8,128)(2,1)S(1)}, bf16[256,2,128]{2,0,1:T(8,128)(2,1)S(1)}, u32[]{:S(2)}, u32[]{:S(2)}) collective-permute-start(bf16[256,2,128]{2,0,1:T(8,128)(2,1)S(1)} %fusion.50), channel_id=1, source_target_pairs={{0,8},{1,9},{2,10},{3,11},{4,12},{5,13},{6,14},{7,15},{8,0},{9,1},... | collective-permute-start | bytes 393224 | tf_op jit(solution)/shard_map/ppermute | solution.py:69
  332.7 8.1 %collective-permute-start.5 = (bf16[256,1,128]{2,0,1:T(8,128)(2,1)S(1)}, bf16[256,1,128]{2,0,1:T(8,128)(2,1)S(1)}, u32[]{:S(2)}, u32[]{:S(2)}) collective-permute-start(bf16[256,1,128]{2,0,1:T(8,128)(2,1)S(1)} %dynamic-slice_convert_fusion.2), channel_id=1, source_target_pairs={{0,4},{1,5},{2,6},{3,7},{4,0},{5,1},{6,2},{7,3},{8,12},{9,13},{10,... | collective-permute-start | bytes 196616 | tf_op jit(solution)/shard_map/ppermute | solution.py:69
  (2 other events, 1.8 us)
